TPU v7x, 256 devices: a 4x2x16 block of a 4x16x16 slice. The times are simulated.
256 devices in a mesh: grp: 2 (over y), fs: 16 (over z), tp: 8 (over x, core).
Axes of the slice: x: 4, y: 2, z: 16, core: 2. Of those that a mesh axis runs over, the one named last changes fastest.
The devices are a block of a 4x16x16 slice.
Arguments:
- tokens: bfloat16 [24576, 2048], P(('grp', 'fs'), 'tp'), parts along dimension 0, may hold values from -6 to 6
- mix_gain: float32 [2048], replicated, may hold values from 0.1 to 1.9
- w_u: float32 [2048, 1024], P('fs', 'tp'), may hold values from -0.125 to 0.125
- w_v: float32 [2048, 1024], P('fs', 'tp'), may hold values from -0.125 to 0.125
- u_scale: float32 [1024], P('tp'), may hold values from 0.5 to 2
- v_scale: float32 [1024], P('tp'), may hold values from 0.5 to 2
- spatial: bfloat16 [8, 128, 128], P('tp'), may hold values from -0.5 to 0.5
- spatial_bias: float32 [8, 128], P('tp'), may hold values from 0.1 to 1.9
- w_mix: float32 [1024, 2048], P('tp', 'fs'), may hold values from -0.1875 to 0.1875
- mix_scale: float32 [1, 2048], P(None, 'fs'), may hold values from 0.5 to 2
- ffn_gain: float32 [2048], replicated, may hold values from 0.1 to 1.9
- w_gate: float32 [2048, 5632], P('fs', 'tp'), may hold values from -0.125 to 0.125
- w_up: float32 [2048, 5632], P('fs', 'tp'), may hold values from -0.125 to 0.125
- gate_scale: float32 [5632], P('tp'), may hold values from 0.5 to 2
- up_scale: float32 [5632], P('tp'), may hold values from 0.5 to 2
- w_down: float32 [5632, 2048], P('tp', 'fs'), may hold values from -0.078125 to 0.078125
- down_scale: float32 [1, 2048], P(None, 'fs'), may hold values from 0.5 to 2
Outputs:
- layer_out: bfloat16 [24576, 2048], P(('grp', 'fs'), 'tp'), parts along dimension 0
There are 2 independent parts, one for each index of `grp`. A program takes and returns all parts, laid end to end along the dimension named above; an argument that names none is the same for every part. Nothing has to cross between parts.
All inputs are finite; a program needn't handle non-finite values.
Results may differ from a plain program's by a relative error of at most 0.024.
Values may be sent and summed in bfloat16 or wider, within the bound.
No kernel may reach another device: no remote copies, remote signals or barrier semaphores. Data moves between devices by JAX's collectives and lax.ppermute only.
A program may use at most 128 MiB of HBM per device.

v0:
```python
import jax
import jax.numpy as jnp
from jax import lax
from jax.sharding import PartitionSpec as P

eps = 1e-06


def sent_to_all(x, axis):
    count = lax.axis_size(axis)
    return lax.all_to_all(jnp.broadcast_to(x[None], (count, *x.shape)), axis, 0, 0, tiled=True)


def in_order(blocks, dim):
    lengths = list(blocks.shape[1:])
    lengths[dim] *= blocks.shape[0]
    return jnp.moveaxis(blocks, 0, dim).reshape(lengths)


def gather_directly(x, axis, dim):
    blocks = sent_to_all(x, axis)
    return in_order(blocks, dim)


def in_one_piece(arrays, axis, dim, along):
    both = jnp.concatenate(arrays, axis=along)
    out, at, done = (lax.all_gather(both, axis, axis=dim, tiled=True), 0, [])
    for a in arrays:
        done.append(lax.slice_in_dim(out, at, at + a.shape[along], axis=along))
        at += a.shape[along]
    return tuple(done)


def norm_rows(shard, gain):
    whole = gather_directly(shard, "tp", 1)
    wide = whole.astype(jnp.float32)
    factor = lax.rsqrt(jnp.mean(wide * wide, axis=1, keepdims=True) + eps)
    return (wide * factor * gain).astype(jnp.bfloat16)


def project_pair(rows, first, second):
    left = first.astype(jnp.bfloat16)
    right = second.astype(jnp.bfloat16)
    pieces = in_one_piece((left, right), "fs", 0, 1)
    return (
        jnp.dot(rows, pieces[0], preferred_element_type=jnp.float32),
        jnp.dot(rows, pieces[1], preferred_element_type=jnp.float32),
    )


def collect_out(weight, scale):
    return (
        lax.all_gather(weight.astype(jnp.bfloat16), "fs", axis=1, tiled=True),
        lax.all_gather(scale.astype(jnp.bfloat16), "fs", axis=1, tiled=True).astype(scale.dtype),
    )


def reduce_out(hidden, weight, scale):
    term = jnp.dot(hidden, weight, preferred_element_type=jnp.float32) * scale
    return lax.psum_scatter(
        term.astype(jnp.bfloat16), "tp", scatter_dimension=1, tiled=True
    ).astype(jnp.float32)


def local(
    tokens,
    mix_gain,
    w_u,
    w_v,
    u_scale,
    v_scale,
    spatial,
    spatial_bias,
    w_mix,
    mix_scale,
    ffn_gain,
    w_gate,
    w_up,
    gate_scale,
    up_scale,
    w_down,
    down_scale,
):
    held = collect_out(w_mix, mix_scale)
    normed_in = norm_rows(tokens, mix_gain)
    u_pre, v_pre = project_pair(normed_in, w_u, w_v)
    u_act = jax.nn.gelu(u_pre * u_scale, approximate=False)
    v_act = jax.nn.gelu(v_pre * v_scale, approximate=False).astype(jnp.bfloat16)
    groups = spatial.shape[0]
    span = spatial.shape[1]
    count = v_act.shape[0]
    blocks = v_act.reshape(count // span, span, groups, v_act.shape[1] // groups)
    later = lax.broadcasted_iota(jnp.int32, (span, span), 0)
    earlier = lax.broadcasted_iota(jnp.int32, (span, span), 1)
    masked = jnp.where((later >= earlier)[None], spatial, jnp.zeros((), jnp.bfloat16))
    spatial_out = jnp.einsum("gts,nsgc->ntgc", masked, blocks, preferred_element_type=jnp.float32)
    spatial_out = spatial_out + spatial_bias.T[None, :, :, None]
    gated = (u_act * spatial_out.reshape(count, v_act.shape[1])).astype(jnp.bfloat16)
    mixed = reduce_out(gated, held[0], held[1])
    resid = (tokens.astype(jnp.float32) + mixed).astype(jnp.bfloat16)
    down_weight, down_factor = collect_out(w_down, down_scale)
    normed_ffn = norm_rows(resid, ffn_gain)
    gate_pre, up_pre = project_pair(normed_ffn, w_gate, w_up)
    act = (jax.nn.silu(gate_pre * gate_scale) * (up_pre * up_scale)).astype(jnp.bfloat16)
    down_sum = reduce_out(act, down_weight, down_factor)
    return (resid.astype(jnp.float32) + down_sum).astype(jnp.bfloat16)


def solution(mesh):
    placed = (
        P(("grp", "fs"), "tp"),
        P(),
        P("fs", "tp"),
        P("fs", "tp"),
        P("tp"),
        P("tp"),
        P("tp", None, None),
        P("tp", None),
        P("tp", "fs"),
        P(None, "fs"),
        P(),
        P("fs", "tp"),
        P("fs", "tp"),
        P("tp"),
        P("tp"),
        P("tp", "fs"),
        P(None, "fs"),
    )
    return jax.shard_map(
        local, mesh=mesh, in_specs=placed, out_specs=P(("grp", "fs"), "tp"), check_vma=False
    )
```

profile of v0, /device:TPU:40, one launch (start us, length us, event | category | flops | bytes accessed | tf_op | source)
XLA Modules:
  0.0 392.7 jit_solution(11202266769531201021)
XLA Ops:
  6.5 1.2 copy.18
  7.7 1.8 broadcast_in_dim.7
  9.6 4.7 %all-to-all-start = ((bf16[8,768,256]{1,2,0:T(8,128)(2,1)}), bf16[8,768,256]{1,2,0:T(8,128)(2,1)S(1)}, u32[]{:S(2)}, u32[]{:S(2)}) async-start(bf16[8,768,256]{1,2,0:T(8,128)(2,1)} %broadcast_in_dim.7), calls=%async_computation | async-start | bytes 6291456 | tf_op jit(solution)/shard_map/all_to_all | solution.py:11
  15.2 48.4 %all_gather.20 = bf16[1,2048]{1,0:T(2,128)(2,1)S(1)} all-gather(bf16[1,128]{1,0:T(2,128)(2,1)S(1)} %convert_element_type.102), channel_id=1, replica_groups=mesh['grp'=2,'fs'=16,'tp'=8] {'fs'}, dimensions={1}, use_global_device_ids=true | all-gather | bytes 4352 | tf_op jit(solution)/shard_map/all_gather | solution.py:54
  63.6 32.5 %all_gather.19 = bf16[128,2048]{1,0:T(8,128)(2,1)} all-gather(bf16[128,128]{1,0:T(8,128)(2,1)S(1)} %convert_element_type.101), channel_id=1, replica_groups=mesh['grp'=2,'fs'=16,'tp'=8] {'fs'}, dimensions={1}, use_global_device_ids=true | all-gather | bytes 557056 | tf_op jit(solution)/shard_map/all_gather | solution.py:53
  96.9 2.4 fusion.3
  99.6 3.9 fusion.21
  103.7 1.7 fusion.18
  105.5 2.6 multiply_convert_fusion.1
  108.3 0.8 pad_maximum_fusion
  109.2 0.7 convert_element_type.115
  110.0 37.4 %reduce-scatter.3.cloned.1.call-done = bf16[768,256]{1,0:T(8,128)(2,1)} async-done(((bf16[768,2048]{1,0:T(8,128)(2,1)}), bf16[768,256]{1,0:T(8,128)(2,1)}) %reduce-scatter.3.cloned.1.call-update) | async-done | bytes 393232 | tf_op jit(solution)/shard_map/reduce_scatter | solution.py:60
  147.4 1.1 add_convert_fusion.1
  148.7 1.9 broadcast_in_dim.9
  150.6 4.0 %all-to-all-start.1 = ((bf16[8,768,256]{1,2,0:T(8,128)(2,1)}), bf16[8,768,256]{1,2,0:T(8,128)(2,1)S(1)}, u32[]{:S(2)}, u32[]{:S(2)}) async-start(bf16[8,768,256]{1,2,0:T(8,128)(2,1)} %broadcast_in_dim.9), calls=%async_computation.2 | async-start | bytes 6291456 | tf_op jit(solution)/shard_map/all_to_all | solution.py:11
  154.7 30.6 %all_gather.23 = bf16[1,2048]{1,0:T(2,128)(2,1)S(1)} all-gather(bf16[1,128]{1,0:T(2,128)(2,1)S(1)} %convert_element_type.116), channel_id=1, replica_groups=mesh['grp'=2,'fs'=16,'tp'=8] {'fs'}, dimensions={1}, use_global_device_ids=true | all-gather | bytes 4352 | tf_op jit(solution)/shard_map/all_gather | solution.py:54
  185.3 7.4 %all-to-all-done.1 = bf16[8,768,256]{1,2,0:T(8,128)(2,1)S(1)} async-done(((bf16[8,768,256]{1,2,0:T(8,128)(2,1)}), bf16[8,768,256]{1,2,0:T(8,128)(2,1)S(1)}, u32[]{:S(2)}, u32[]{:S(2)}) %all-to-all-start.1) | async-done | bytes 3145760 | tf_op jit(solution)/shard_map/all_to_all | solution.py:11
  193.5 2.5 fusion.1
  195.9 59.6 %all-gather.6.cloned.1.call-done = bf16[2048,1408]{0,1:T(8,128)(2,1)} async-done(((bf16[128,1408]{0,1:T(8,128)(2,1)}), bf16[2048,1408]{0,1:T(8,128)(2,1)}) %all-gather.6.cloned.1.call-update) | async-done | bytes 5767184 | tf_op jit(solution)/shard_map/all_gather | solution.py:27
  255.5 6.6 %fusion.4 = f32[768,704]{0,1:T(8,128)} fusion(bf16[768,2048]{0,1:T(8,128)(2,1)} %fusion.1, bf16[2048,1408]{0,1:T(8,128)(2,1)} %all-gather.6.cloned.1.call-done), kind=kOutput, calls=%fused_computation.10 | convolution fusion | flops 2214592512 | bytes 8192000 | tf_op jit(solution)/shard_map/dot_general | solution.py:47
  262.1 72.1 %all-gather.8.cloned.1.call-done = bf16[704,2048]{1,0:T(8,128)(2,1)} async-done(((bf16[704,128]{1,0:T(8,128)(2,1)}), bf16[704,2048]{1,0:T(8,128)(2,1)}) %all-gather.8.cloned.1.call-update) | async-done | bytes 2883600 | tf_op jit(solution)/shard_map/all_gather | solution.py:53
  334.2 11.6 %multiply_convert_fusion = bf16[768,2048]{1,0:T(8,128)(2,1)} fusion(bf16[704,2048]{1,0:T(8,128)(2,1)} %all-gather.8.cloned.1.call-done, f32[2048]{0:T(1024)S(1)} %bitcast.42, f32[768,704]{0,1:T(8,128)} %fusion.4, bf16[768,2048]{0,1:T(8,128)(2,1)S(1)} %copy-done, bf16[2048,1408]{0,1:T(8,128)(2,1)} %all-gather.6.cloned.1.call-done, f32[704]{0:T(1024)S(1)} %copy-done.15, ...), kind=kOutput, calls=%fused_computation.6 | convolution fusion | flops 4436656128 | bytes 14235136 | tf_op jit(solution)/shard_map/dot_general | solution.py:59
  345.9 38.4 %reduce-scatter.5.cloned.1.call-done = bf16[768,256]{1,0:T(8,128)(2,1)} async-done(((bf16[768,2048]{1,0:T(8,128)(2,1)}), bf16[768,256]{1,0:T(8,128)(2,1)}) %reduce-scatter.5.cloned.1.call-update) | async-done | bytes 393232 | tf_op jit(solution)/shard_map/reduce_scatter | solution.py:60
  384.3 1.8 add_convert_fusion
  (70 shorter events, 3.4 us)
Async XLA Ops:
  9.6 4.8 %copy-start.7 = (f32[128,128]{1,0:T(8,128)S(1)}, f32[128,128]{1,0:T(8,128)}, u32[]{:S(2)}) copy-start(f32[128,128]{1,0:T(8,128)} %param.19) | copy-start | bytes 196612
  9.6 4.8 %copy-start.8 = (f32[128,128]{1,0:T(8,128)S(1)}, f32[128,128]{1,0:T(8,128)}, u32[]{:S(2)}) copy-start(f32[128,128]{1,0:T(8,128)} %param.20) | copy-start | bytes 196612
  9.6 5.6 %copy-start.17 = (f32[1,128]{1,0:T(1,128)S(1)}, f32[1,128]{1,0:T(1,128)}, u32[]{:S(2)}) copy-start(f32[1,128]{1,0:T(1,128)} %param.26) | copy-start | bytes 1540
  9.6 54.0 %copy-start.9 = (f32[128,128]{1,0:T(8,128)S(1)}, f32[128,128]{1,0:T(8,128)}, u32[]{:S(2)}) copy-start(f32[128,128]{1,0:T(8,128)} %param.25) | copy-start | bytes 196612
  9.6 86.6 %all-to-all-start = ((bf16[8,768,256]{1,2,0:T(8,128)(2,1)}), bf16[8,768,256]{1,2,0:T(8,128)(2,1)S(1)}, u32[]{:S(2)}, u32[]{:S(2)}) async-start(bf16[8,768,256]{1,2,0:T(8,128)(2,1)} %broadcast_in_dim.7), calls=%async_computation | async-start | bytes 6291456 | tf_op jit(solution)/shard_map/all_to_all | solution.py:11
  14.3 82.5 %copy-start.11 = (f32[2048]{0:T(1024)S(1)}, f32[2048]{0:T(1024)}, u32[]{:S(2)}) copy-start(f32[2048]{0:T(1024)} %param.18) | copy-start | bytes 24580
  14.3 85.2 %all-gather.4.cloned.1.call-start = ((), (), s32[]{:S(2)}) async-start(), calls=%async_computation.4 | async-start | bytes 1114112 | tf_op jit(solution)/shard_map/all_gather | solution.py:27
  15.1 132.3 %reduce-scatter.3.cloned.1.call-start = ((), (), s32[]{:S(2)}) async-start(), calls=%async_computation.5 | async-start | bytes 3538944 | tf_op jit(solution)/shard_map/reduce_scatter | solution.py:60
  99.3 4.2 %copy-start.10 = (bf16[1,128,128]{2,1,0:T(8,128)(2,1)S(1)}, bf16[1,128,128]{2,1,0:T(8,128)(2,1)}, u32[]{:S(2)}) copy-start(bf16[1,128,128]{2,1,0:T(8,128)(2,1)} %param.23) | copy-start | bytes 98308
  99.3 4.2 %copy-start.13 = (f32[1,128]{1,0:T(1,128)S(1)}, f32[1,128]{1,0:T(1,128)}, u32[]{:S(2)}) copy-start(f32[1,128]{1,0:T(1,128)} %param.24) | copy-start | bytes 1540
  99.3 4.4 %copy-start.1 = (bf16[768,2048]{0,1:T(8,128)(2,1)S(1)}, bf16[768,2048]{0,1:T(8,128)(2,1)}, u32[]{:S(2)}) copy-start(bf16[768,2048]{0,1:T(8,128)(2,1)} %fusion.3) | copy-start | bytes 9437188
  99.3 4.4 %copy-start.19 = (f32[128]{0:T(128)S(1)}, f32[128]{0:T(128)}, u32[]{:S(2)}) copy-start(f32[128]{0:T(128)} %param.21) | copy-start | bytes 1540
  99.6 4.1 %copy-start.14 = (bf16[2048,256]{1,0:T(8,128)(2,1)S(1)}, bf16[2048,256]{1,0:T(8,128)(2,1)}, u32[]{:S(2)}) copy-start(bf16[2048,256]{1,0:T(8,128)(2,1)} %all-gather.4.cloned.1.call-done) | copy-start | bytes 3145732
  105.4 2.8 copy-start.5
  108.1 39.3 %copy-start.3 = (bf16[768,256]{1,0:T(8,128)(2,1)S(1)}, bf16[768,256]{1,0:T(8,128)(2,1)}, u32[]{:S(2)}) copy-start(bf16[768,256]{1,0:T(8,128)(2,1)} %param.17) | copy-start | bytes 1179652
  108.2 147.4 %all-gather.6.cloned.1.call-start = ((), (), s32[]{:S(2)}) async-start(), calls=%async_computation.6 | async-start | bytes 6127616 | tf_op jit(solution)/shard_map/all_gather | solution.py:27
  109.1 225.1 %all-gather.8.cloned.1.call-start = ((), (), s32[]{:S(2)}) async-start(), calls=%async_computation.7 | async-start | bytes 3063808 | tf_op jit(solution)/shard_map/all_gather | solution.py:53
  150.6 4.1 %copy-start.20 = (f32[1,128]{1,0:T(1,128)S(1)}, f32[1,128]{1,0:T(1,128)}, u32[]{:S(2)}) copy-start(f32[1,128]{1,0:T(1,128)} %param.33) | copy-start | bytes 1540
  150.6 42.2 %all-to-all-start.1 = ((bf16[8,768,256]{1,2,0:T(8,128)(2,1)}), bf16[8,768,256]{1,2,0:T(8,128)(2,1)S(1)}, u32[]{:S(2)}, u32[]{:S(2)}) async-start(bf16[8,768,256]{1,2,0:T(8,128)(2,1)} %broadcast_in_dim.9), calls=%async_computation.2 | async-start | bytes 6291456 | tf_op jit(solution)/shard_map/all_to_all | solution.py:11
  154.6 38.9 %copy-start.12 = (f32[2048]{0:T(1024)S(1)}, f32[2048]{0:T(1024)}, u32[]{:S(2)}) copy-start(f32[2048]{0:T(1024)} %param.27) | copy-start | bytes 24580
  154.6 229.7 %reduce-scatter.5.cloned.1.call-start = ((), (), s32[]{:S(2)}) async-start(), calls=%async_computation.8 | async-start | bytes 3538944 | tf_op jit(solution)/shard_map/reduce_scatter | solution.py:60
  195.9 138.3 %copy-start = (bf16[768,2048]{0,1:T(8,128)(2,1)S(1)}, bf16[768,2048]{0,1:T(8,128)(2,1)}, u32[]{:S(2)}) copy-start(bf16[768,2048]{0,1:T(8,128)(2,1)} %fusion.1) | copy-start | bytes 9437188
  195.9 138.3 %copy-start.15 = (f32[704]{0:T(1024)S(1)}, f32[704]{0:T(1024)}, u32[]{:S(2)}) copy-start(f32[704]{0:T(1024)} %param.31) | copy-start | bytes 8452
  195.9 138.3 %copy-start.16 = (f32[704]{0:T(1024)S(1)}, f32[704]{0:T(1024)}, u32[]{:S(2)}) copy-start(f32[704]{0:T(1024)} %param.30) | copy-start | bytes 8452
  (4 other events, 8.4 us)
Sparse Core Ops, SparseCore 0:
  16.9 82.5 all-gather.3
  108.3 39.0 reduce-scatter.2
  149.1 106.3 all-gather.5
  257.1 77.0 all-gather.7
  346.0 38.2 reduce-scatter.4
where the time goes:
time: 393 us
  waiting for transfers between devices  216 us (55%)
  blocking collectives  111 us (28%)
  matrix products  26.5 us (7%)
  between operations  13.5 us (3%)
  other arithmetic  11.4 us (3%)
  starting transfers between devices  9.04 us (2%)
  local copies, waits for them, and re-layouts  5.15 us (1%)
    all_gather x2, blocking collectives, collect_out(): lax.all_gather(scale.astype(jnp.bfloat16), 'fs', axis=1, tiled=True)  79 us
    reduce_scatter x2, waiting for transfers between devices, reduce_out(): lax.psum_scatter(term.astype(jnp.bfloat16), 'tp', scatter_dimension=1, ti...  75.9 us
    all_gather x1, waiting for transfers between devices, collect_out(): lax.all_gather(weight.astype(jnp.bfloat16), 'fs', axis=1, tiled=True)  72.1 us
    all_gather x2, waiting for transfers between devices, in_one_piece(): out, at, done = (lax.all_gather(both, axis, axis=dim, tiled=True), 0, [])  59.9 us
    all_gather x1, blocking collectives, collect_out(): lax.all_gather(weight.astype(jnp.bfloat16), 'fs', axis=1, tiled=True)  32.5 us
    dot_general x2, matrix products, reduce_out(): term = jnp.dot(hidden, weight, preferred_element_type=jnp.float32) * scale  14.2 us
    dot_general x2, matrix products, project_pair(): jnp.dot(rows, pieces[1], preferred_element_type=jnp.float32)  10.4 us
    all_to_all x2, starting transfers between devices, sent_to_all(): lax.all_to_all(jnp.broadcast_to(x[None], (count, *x.shape)), axis, 0, 0,...  8.72 us
  transfers between devices with their start and end apart: 7, of which 6 were waited for; matrix products, arithmetic and copies ran while one was open for 5% of the time, Pallas kernels for 0%

commit v1 on v0

--- a/solution.py
+++ b/solution.py
@@ -50,7 +50,12 @@
 
 def collect_out(weight, scale):
     return (
-        lax.all_gather(weight.astype(jnp.bfloat16), "fs", axis=1, tiled=True),
+        jnp.concatenate(
+            lax.all_to_all(
+                jnp.stack([weight.astype(jnp.bfloat16)] * lax.axis_size("fs")), "fs", 0, 0
+            ),
+            axis=1,
+        ),
         lax.all_gather(scale.astype(jnp.bfloat16), "fs", axis=1, tiled=True).astype(scale.dtype),
     )
 

time: 393 us -> 456 us (1.16)
  blocking collectives: 111 us -> 218 us
  waiting for transfers between devices: 216 us -> 139 us
  starting transfers between devices: 9.04 us -> 34.4 us
    all_gather x2, blocking collectives: 79 us -> 218 us  [collect_out(): lax.all_gather(scale.astype(jnp.bfloat16), 'fs', axis=1, tiled=True)]
    all_gather x1 -> x0, waiting for transfers between devices: 72.1 us -> none  [collect_out(): lax.all_gather(weight.astype(jnp.bfloat16), 'fs', axis=1, tiled=True)]
    all_gather x2, waiting for transfers between devices: 59.9 us -> 26.7 us  [in_one_piece(): out, at, done = (lax.all_gather(both, axis, axis=dim, tiled=True), 0, [])]
    all_gather x1 -> x0, blocking collectives: 32.5 us -> none  [collect_out(): lax.all_gather(weight.astype(jnp.bfloat16), 'fs', axis=1, tiled=True)]
    all_to_all x2, waiting for transfers between devices: 7.44 us -> 33.6 us  [sent_to_all(): lax.all_to_all(jnp.broadcast_to(x[None], (count, *x.shape)), axis, 0, 0,...]
    all_to_all x0 -> x2, starting transfers between devices: none -> 25.5 us  [collect_out(): lax.all_to_all(jnp.stack([weight.astype(jnp.bfloat16)] * lax.axis_size('f...]
  transfers between devices with their start and end apart: 7 -> 8, of which waited for: 6 -> 4; matrix products, arithmetic and copies ran while one was open for 5% -> 6% of each run, Pallas kernels for 0% -> 0%
where the time goes in v1:
time: 456 us
  blocking collectives  218 us (48%)
  waiting for transfers between devices  139 us (30%)
  starting transfers between devices  34.4 us (8%)
  matrix products  27.6 us (6%)
  other arithmetic  14.3 us (3%)
  between operations  13.4 us (3%)
  local copies, waits for them, and re-layouts  9.25 us (2%)
    all_gather x2, blocking collectives, collect_out(): lax.all_gather(scale.astype(jnp.bfloat16), 'fs', axis=1, tiled=True)  218 us
    reduce_scatter x2, waiting for transfers between devices, reduce_out(): lax.psum_scatter(term.astype(jnp.bfloat16), 'tp', scatter_dimension=1, ti...  78.2 us
    all_to_all x2, waiting for transfers between devices, sent_to_all(): lax.all_to_all(jnp.broadcast_to(x[None], (count, *x.shape)), axis, 0, 0,...  33.6 us
    all_gather x2, waiting for transfers between devices, in_one_piece(): out, at, done = (lax.all_gather(both, axis, axis=dim, tiled=True), 0, [])  26.7 us
    all_to_all x2, starting transfers between devices, collect_out(): lax.all_to_all(jnp.stack([weight.astype(jnp.bfloat16)] * lax.axis_size('f...  25.5 us
    dot_general x2, matrix products, reduce_out(): term = jnp.dot(hidden, weight, preferred_element_type=jnp.float32) * scale  15.2 us
    dot_general x2, matrix products, project_pair(): jnp.dot(rows, pieces[1], preferred_element_type=jnp.float32)  10.4 us
  transfers between devices with their start and end apart: 8, of which 4 were waited for; matrix products, arithmetic and copies ran while one was open for 6% of the time, Pallas kernels for 0%

profile of v1, /device:TPU:40, one launch (start us, length us, event | category | flops | bytes accessed | tf_op | source)
XLA Modules:
  0.0 455.5 jit_solution(3014302320409553870)
XLA Ops:
  6.5 1.2 copy.21
  7.7 1.8 broadcast_in_dim.7
  9.6 4.7 %all-to-all-start = ((bf16[8,768,256]{1,2,0:T(8,128)(2,1)}), bf16[8,768,256]{1,2,0:T(8,128)(2,1)S(1)}, u32[]{:S(2)}, u32[]{:S(2)}) async-start(bf16[8,768,256]{1,2,0:T(8,128)(2,1)} %broadcast_in_dim.7), calls=%async_computation | async-start | bytes 6291456 | tf_op jit(solution)/shard_map/all_to_all | solution.py:11
  15.1 48.4 %all_gather.13 = bf16[1,2048]{1,0:T(2,128)(2,1)S(1)} all-gather(bf16[1,128]{1,0:T(2,128)(2,1)S(1)} %convert_element_type.102), channel_id=1, replica_groups=mesh['grp'=2,'fs'=16,'tp'=8] {'fs'}, dimensions={1}, use_global_device_ids=true | all-gather | bytes 4352 | tf_op jit(solution)/shard_map/all_gather | solution.py:59
  64.6 13.0 %all-to-all-start.1 = ((bf16[16,128,128]{1,2,0:T(8,128)(2,1)}), bf16[16,128,128]{1,2,0:T(8,128)(2,1)}, u32[]{:S(2)}, u32[]{:S(2)}) async-start(bf16[16,128,128]{1,2,0:T(8,128)(2,1)} %stack.4), calls=%async_computation.1 | async-start | bytes 1048576 | tf_op jit(solution)/shard_map/all_to_all | solution.py:54
  78.4 2.4 fusion.3
  80.8 26.7 %all-gather.3.cloned.1.call-done = bf16[2048,256]{1,0:T(8,128)(2,1)} async-done(((bf16[128,256]{1,0:T(8,128)(2,1)}), bf16[2048,256]{1,0:T(8,128)(2,1)}) %all-gather.3.cloned.1.call-update) | async-done | bytes 1048592 | tf_op jit(solution)/shard_map/all_gather | solution.py:27
  107.5 3.8 fusion.23
  111.5 1.7 fusion.20
  113.3 3.7 multiply_convert_fusion.1
  117.1 40.1 %reduce-scatter.3.cloned.1.call-done = bf16[768,256]{1,0:T(8,128)(2,1)} async-done(((bf16[768,2048]{1,0:T(8,128)(2,1)}), bf16[768,256]{1,0:T(8,128)(2,1)}) %reduce-scatter.3.cloned.1.call-update) | async-done | bytes 393232 | tf_op jit(solution)/shard_map/reduce_scatter | solution.py:65
  157.2 1.1 add_convert_fusion.1
  158.4 1.9 broadcast_in_dim.9
  160.3 3.9 all-to-all-start.2
  167.1 1.7 convert_element_type.115
  168.8 33.6 %all-to-all-done.2 = bf16[8,768,256]{1,2,0:T(8,128)(2,1)S(1)} async-done(((bf16[8,768,256]{1,2,0:T(8,128)(2,1)}), bf16[8,768,256]{1,2,0:T(8,128)(2,1)S(1)}, u32[]{:S(2)}, u32[]{:S(2)}) %all-to-all-start.2) | async-done | bytes 3145760 | tf_op jit(solution)/shard_map/all_to_all | solution.py:11
  202.4 3.1 stack.5
  205.5 12.5 %all-to-all-start.3 = ((bf16[16,704,128]{2,1,0:T(8,128)(2,1)}), bf16[16,704,128]{2,1,0:T(8,128)(2,1)}, u32[]{:S(2)}, u32[]{:S(2)}) async-start(bf16[16,704,128]{2,1,0:T(8,128)(2,1)} %stack.5), calls=%async_computation.4 | async-start | bytes 5767168 | tf_op jit(solution)/shard_map/all_to_all | solution.py:54
  218.1 169.6 %all_gather.15 = bf16[1,2048]{1,0:T(2,128)(2,1)S(1)} all-gather(bf16[1,128]{1,0:T(2,128)(2,1)S(1)} %convert_element_type.116), channel_id=1, replica_groups=mesh['grp'=2,'fs'=16,'tp'=8] {'fs'}, dimensions={1}, use_global_device_ids=true | all-gather | bytes 4352 | tf_op jit(solution)/shard_map/all_gather | solution.py:59
  388.4 2.5 fusion.1
  390.8 6.6 %fusion.6 = f32[768,704]{0,1:T(8,128)} fusion(bf16[768,2048]{0,1:T(8,128)(2,1)} %fusion.1, bf16[2048,1408]{0,1:T(8,128)(2,1)} %all-gather.5.cloned.1.call-done), kind=kOutput, calls=%fused_computation.12 | convolution fusion | flops 2214592512 | bytes 8192000 | tf_op jit(solution)/shard_map/dot_general | solution.py:47
  397.5 11.5 %multiply_convert_fusion = bf16[768,2048]{1,0:T(8,128)(2,1)} fusion(f32[2048]{0:T(1024)S(1)} %bitcast.52, f32[768,704]{0,1:T(8,128)} %fusion.6, bf16[768,2048]{0,1:T(8,128)(2,1)S(1)} %copy-done, bf16[2048,1408]{0,1:T(8,128)(2,1)} %all-gather.5.cloned.1.call-done, f32[704]{0:T(1024)S(1)} %copy-done.11, f32[704]{0:T(1024)S(1)} %copy-done.12, ...), kind=kOutput, calls=%fused_computation.6 | convolution fusion | flops 4436656128 | bytes 14235136 | tf_op jit(solution)/shard_map/dot_general | solution.py:64
  409.1 38.1 %reduce-scatter.5.cloned.1.call-done = bf16[768,256]{1,0:T(8,128)(2,1)} async-done(((bf16[768,2048]{1,0:T(8,128)(2,1)}), bf16[768,256]{1,0:T(8,128)(2,1)}) %reduce-scatter.5.cloned.1.call-update) | async-done | bytes 393232 | tf_op jit(solution)/shard_map/reduce_scatter | solution.py:65
  447.2 1.8 add_convert_fusion
  (65 shorter events, 6.8 us)
Async XLA Ops:
  9.6 4.8 %copy-start.3 = (f32[128,128]{1,0:T(8,128)S(1)}, f32[128,128]{1,0:T(8,128)}, u32[]{:S(2)}) copy-start(f32[128,128]{1,0:T(8,128)} %param.19) | copy-start | bytes 196612
  9.6 4.8 %copy-start.4 = (f32[128,128]{1,0:T(8,128)S(1)}, f32[128,128]{1,0:T(8,128)}, u32[]{:S(2)}) copy-start(f32[128,128]{1,0:T(8,128)} %param.20) | copy-start | bytes 196612
  9.6 5.6 %copy-start.13 = (f32[1,128]{1,0:T(1,128)S(1)}, f32[1,128]{1,0:T(1,128)}, u32[]{:S(2)}) copy-start(f32[1,128]{1,0:T(1,128)} %param.26) | copy-start | bytes 1540
  9.6 53.9 %copy-start.5 = (f32[128,128]{1,0:T(8,128)S(1)}, f32[128,128]{1,0:T(8,128)}, u32[]{:S(2)}) copy-start(f32[128,128]{1,0:T(8,128)} %param.25) | copy-start | bytes 196612
  9.6 54.1 %all-to-all-start = ((bf16[8,768,256]{1,2,0:T(8,128)(2,1)}), bf16[8,768,256]{1,2,0:T(8,128)(2,1)S(1)}, u32[]{:S(2)}, u32[]{:S(2)}) async-start(bf16[8,768,256]{1,2,0:T(8,128)(2,1)} %broadcast_in_dim.7), calls=%async_computation | async-start | bytes 6291456 | tf_op jit(solution)/shard_map/all_to_all | solution.py:11
  14.3 64.1 %copy-start.7 = (f32[2048]{0:T(1024)S(1)}, f32[2048]{0:T(1024)}, u32[]{:S(2)}) copy-start(f32[2048]{0:T(1024)} %param.18) | copy-start | bytes 24580
  14.3 93.2 %all-gather.3.cloned.1.call-start = ((), (), s32[]{:S(2)}) async-start(), calls=%async_computation.6 | async-start | bytes 1114112 | tf_op jit(solution)/shard_map/all_gather | solution.py:27
  64.6 48.7 %all-to-all-start.1 = ((bf16[16,128,128]{1,2,0:T(8,128)(2,1)}), bf16[16,128,128]{1,2,0:T(8,128)(2,1)}, u32[]{:S(2)}, u32[]{:S(2)}) async-start(bf16[16,128,128]{1,2,0:T(8,128)(2,1)} %stack.4), calls=%async_computation.1 | async-start | bytes 1048576 | tf_op jit(solution)/shard_map/all_to_all | solution.py:54
  77.6 79.6 %reduce-scatter.3.cloned.1.call-start = ((), (), s32[]{:S(2)}) async-start(), calls=%async_computation.7 | async-start | bytes 3538944 | tf_op jit(solution)/shard_map/reduce_scatter | solution.py:65
  78.4 29.1 %copy-start.14 = (f32[128]{0:T(128)S(1)}, f32[128]{0:T(128)}, u32[]{:S(2)}) copy-start(f32[128]{0:T(128)} %param.22) | copy-start | bytes 1540
  80.8 30.5 %copy-start.6 = (bf16[1,128,128]{2,1,0:T(8,128)(2,1)S(1)}, bf16[1,128,128]{2,1,0:T(8,128)(2,1)}, u32[]{:S(2)}) copy-start(bf16[1,128,128]{2,1,0:T(8,128)(2,1)} %param.23) | copy-start | bytes 98308
  80.8 30.5 %copy-start.9 = (f32[1,128]{1,0:T(1,128)S(1)}, f32[1,128]{1,0:T(1,128)}, u32[]{:S(2)}) copy-start(f32[1,128]{1,0:T(1,128)} %param.24) | copy-start | bytes 1540
  80.8 30.7 %copy-start.1 = (bf16[768,2048]{0,1:T(8,128)(2,1)S(1)}, bf16[768,2048]{0,1:T(8,128)(2,1)}, u32[]{:S(2)}) copy-start(bf16[768,2048]{0,1:T(8,128)(2,1)} %fusion.3) | copy-start | bytes 9437188
  80.8 30.7 %copy-start.15 = (f32[128]{0:T(128)S(1)}, f32[128]{0:T(128)}, u32[]{:S(2)}) copy-start(f32[128]{0:T(128)} %param.21) | copy-start | bytes 1540
  113.3 43.9 %copy-start.2 = (bf16[768,256]{1,0:T(8,128)(2,1)S(1)}, bf16[768,256]{1,0:T(8,128)(2,1)}, u32[]{:S(2)}) copy-start(bf16[768,256]{1,0:T(8,128)(2,1)} %param.17) | copy-start | bytes 1179652
  160.3 42.0 %all-to-all-start.2 = ((bf16[8,768,256]{1,2,0:T(8,128)(2,1)}), bf16[8,768,256]{1,2,0:T(8,128)(2,1)S(1)}, u32[]{:S(2)}, u32[]{:S(2)}) async-start(bf16[8,768,256]{1,2,0:T(8,128)(2,1)} %broadcast_in_dim.9), calls=%async_computation.3 | async-start | bytes 6291456 | tf_op jit(solution)/shard_map/all_to_all | solution.py:11
  164.2 226.6 %all-gather.5.cloned.1.call-start = ((), (), s32[]{:S(2)}) async-start(), calls=%async_computation.8 | async-start | bytes 6127616 | tf_op jit(solution)/shard_map/all_gather | solution.py:27
  205.5 12.6 %copy-start.16 = (f32[1,128]{1,0:T(1,128)S(1)}, f32[1,128]{1,0:T(1,128)}, u32[]{:S(2)}) copy-start(f32[1,128]{1,0:T(1,128)} %param.33) | copy-start | bytes 1540
  205.5 182.9 %copy-start.8 = (f32[2048]{0:T(1024)S(1)}, f32[2048]{0:T(1024)}, u32[]{:S(2)}) copy-start(f32[2048]{0:T(1024)} %param.27) | copy-start | bytes 24580
  205.5 192.0 %all-to-all-start.3 = ((bf16[16,704,128]{2,1,0:T(8,128)(2,1)}), bf16[16,704,128]{2,1,0:T(8,128)(2,1)}, u32[]{:S(2)}, u32[]{:S(2)}) async-start(bf16[16,704,128]{2,1,0:T(8,128)(2,1)} %stack.5), calls=%async_computation.4 | async-start | bytes 5767168 | tf_op jit(solution)/shard_map/all_to_all | solution.py:54
  218.0 229.2 %reduce-scatter.5.cloned.1.call-start = ((), (), s32[]{:S(2)}) async-start(), calls=%async_computation.9 | async-start | bytes 3538944 | tf_op jit(solution)/shard_map/reduce_scatter | solution.py:65
  390.8 6.7 %copy-start = (bf16[768,2048]{0,1:T(8,128)(2,1)S(1)}, bf16[768,2048]{0,1:T(8,128)(2,1)}, u32[]{:S(2)}) copy-start(bf16[768,2048]{0,1:T(8,128)(2,1)} %fusion.1) | copy-start | bytes 9437188
  390.8 6.7 %copy-start.11 = (f32[704]{0:T(1024)S(1)}, f32[704]{0:T(1024)}, u32[]{:S(2)}) copy-start(f32[704]{0:T(1024)} %param.31) | copy-start | bytes 8452
  390.8 6.7 %copy-start.12 = (f32[704]{0:T(1024)S(1)}, f32[704]{0:T(1024)}, u32[]{:S(2)}) copy-start(f32[704]{0:T(1024)} %param.30) | copy-start | bytes 8452
  (1 other events, 4.0 us)
Sparse Core Ops, SparseCore 0:
  16.9 90.5 all-gather.2
  117.2 39.9 reduce-scatter.2
  167.2 222.7 all-gather.4
  409.2 37.8 reduce-scatter.4
